TPU v7x, 512 devices: a whole 4x4x16 slice. The times are simulated.
512 devices in a mesh: sp: 128 (over z, x, core), tp: 4 (over y).
Axes of the slice: x: 4, y: 4, z: 16, core: 2. Of those that a mesh axis runs over, the one named last changes fastest.
Arguments:
- tokens: bfloat16 [16384, 2048], P('sp', 'tp'), may hold values from -6 to 6
- conv_value_weight: bfloat16 [2048, 1024], P('sp', 'tp'), may hold values from -0.125 to 0.125
- conv_gate_weight: bfloat16 [2048, 1024], P('sp', 'tp'), may hold values from -0.125 to 0.125
- conv_kernel: bfloat16 [31, 1024], P(None, 'tp'), may hold values from -16 to 16
- conv_norm_gain: float32 [1024], P('tp'), may hold values from 0.1 to 1.9
- query_weight: bfloat16 [2048, 2048], P('sp', 'tp'), may hold values from -0.125 to 0.125
- key_weight: bfloat16 [2048, 2048], P('sp', 'tp'), may hold values from -0.125 to 0.125
- value_weight: bfloat16 [2048, 2048], P('sp', 'tp'), may hold values from -0.125 to 0.125
- input_gate_weight: bfloat16 [2048, 8], P(None, 'tp'), may hold values from -0.125 to 0.125
- forget_gate_weight: bfloat16 [2048, 8], P(None, 'tp'), may hold values from -0.125 to 0.125
- input_offset: float32 [16384, 8], P('sp', 'tp'), may hold values from -4 to 210
- forget_offset: float32 [16384, 8], P('sp', 'tp'), may hold values from 0 to 30
- memory_norm_gain: float32 [2048], P('tp'), may hold values from 0.1 to 1.9
- conv_out_weight: bfloat16 [1024, 2048], P('tp', 'sp'), may hold values from -0.3125 to 0.3125
- memory_out_weight: bfloat16 [2048, 2048], P('tp', 'sp'), may hold values from -0.125 to 0.125
Outputs:
- mixed: bfloat16 [16384, 2048], P('sp', 'tp')
All inputs are finite; a program needn't handle non-finite values.
Results may differ from a plain program's by a relative error of at most 0.03.
Values may be sent and summed in bfloat16 or wider, within the bound.
No kernel may reach another device: no remote copies, remote signals or barrier semaphores. Data moves between devices by JAX's collectives and lax.ppermute only.
A program may use at most 128 MiB of HBM per device.

v0:
```python
import jax
import jax.numpy as jnp
from jax import lax
from jax.sharding import Mesh
from jax.sharding import PartitionSpec as P

BLOCK = 64
SP = ("sp_0", "sp_1", "sp_2")
EPS = 1e-06
LOWEST_LEVEL = -1e30


def in_order(blocks, dim):
    blocks = jnp.moveaxis(blocks, 0, dim)
    lengths = blocks.shape
    return blocks.reshape(*lengths[:dim], lengths[dim] * lengths[dim + 1], *lengths[dim + 2 :])


def copy_for_each(shard, axis):
    copies = jnp.broadcast_to(shard, (lax.axis_size(axis), *shard.shape))
    return lax.all_to_all(copies, axis, split_axis=0, concat_axis=0, tiled=True)


def gather_directly(shard, axis, dim):
    return in_order(copy_for_each(shard, axis), dim)


def sent_together(arrays, axis, dim, along):
    ends, at = ([], 0)
    for a in arrays[:-1]:
        at += a.shape[along]
        ends.append(at)
    both = jnp.concatenate(arrays, axis=along)
    return tuple(jnp.split(lax.all_gather(both, axis, axis=dim, tiled=True), ends, axis=along))


def shifted_2(value, axis, steps):
    count = lax.axis_size(axis)
    leading, last = (max(0, -steps), min(count, count - steps))
    return lax.ppermute(value, axis, [(source, source + steps) for source in range(leading, last)])


def neutral_like(shard, identity):
    return jax.tree.map(
        lambda a, e: jnp.broadcast_to(jnp.asarray(e, a.dtype), a.shape), shard, identity
    )


def entering(shard, axes, combine, identity):
    before = start = neutral_like(shard, identity)
    total = shard
    for axis in reversed(axes):
        devices, position = (lax.axis_size(axis), lax.axis_index(axis))
        pieces = jax.tree.map(
            lambda part, kind: lax.all_gather(part.astype(kind), axis),
            total,
            (jnp.bfloat16, jnp.bfloat16, jnp.bfloat16, jnp.bfloat16),
        )
        inside, total = (start, start)
        for k in range(devices):
            passed = k < position
            total = combine(
                total, jax.tree.map(lambda part, own: part[k].astype(own.dtype), pieces, shard)
            )
            inside = jax.tree.map(lambda new, old: jnp.where(passed, new, old), total, inside)
        before = combine(inside, before)
    return before


def of_everyone(shard, axis):
    return copy_for_each(shard, axis).sum(axis=0)


def turned_gather(arrays, axis, dims):
    turned = [jnp.moveaxis(a, dim, 0) for a, dim in zip(arrays, dims)]
    both = jnp.concatenate([t.reshape(len(t), -1) for t in turned], axis=1)
    out, at, finished = (lax.all_gather(both, axis, axis=0, tiled=True), 0, [])
    for t, dim in zip(turned, dims):
        share = out[:, at : at + t[0].size].reshape(-1, *t.shape[1:])
        finished.append(jnp.moveaxis(share, 0, dim))
        at += t[0].size
    return tuple(finished)


def cut_along(shard, dim, devices):
    before, after = (shard.shape[:dim], shard.shape[dim + 1 :])
    return jnp.moveaxis(shard.reshape(*before, devices, -1, *after), dim, 0)


def sum_at_owner(shard, axis, dim):
    blocks = cut_along(shard, dim, lax.axis_size(axis))
    arrived = lax.all_to_all(blocks, axis, split_axis=0, concat_axis=0, tiled=True)
    return arrived.astype(jnp.float32).sum(axis=0)


def block_step(carry, inputs):
    state, normal, level = carry
    query, key, value, gate_in, forget_log = inputs
    length = gate_in.shape[-1]
    scale = query.shape[-1] ** (-0.5)
    causal = jnp.tril(jnp.ones((length, length), dtype=bool))
    within = jnp.cumsum(forget_log, axis=-1)
    log_weight = within[:, :, None] - within[:, None, :] + gate_in[:, None, :]
    log_weight = jnp.where(causal, log_weight, -jnp.inf)
    carried = within + level[:, None]
    top = jnp.maximum(carried, jnp.max(log_weight, axis=-1))
    weight = jnp.exp(log_weight - top[:, :, None])
    carried_weight = jnp.exp(carried - top) * scale
    scores = jnp.einsum("htd,hsd->hts", query, key, preferred_element_type=jnp.float32) * (
        scale * weight
    )
    numer = jnp.einsum(
        "hts,hse->hte", scores.astype(jnp.bfloat16), value, preferred_element_type=jnp.float32
    )
    numer = numer + carried_weight[:, :, None] * jnp.einsum(
        "hed,htd->hte", state.astype(jnp.bfloat16), query, preferred_element_type=jnp.float32
    )
    denom = jnp.sum(scores, axis=-1) + carried_weight * jnp.einsum(
        "hd,htd->ht", normal.astype(jnp.bfloat16), query, preferred_element_type=jnp.float32
    )
    result = numer / jnp.maximum(jnp.abs(denom), 1.0)[:, :, None]
    last = within[:, -1]
    end_log = last[:, None] - within + gate_in
    new_level = jnp.maximum(last + level, jnp.max(end_log, axis=-1))
    keep = jnp.exp(last + level - new_level)
    fresh = jnp.exp(end_log - new_level[:, None])
    scaled_key = (fresh[:, :, None] * key).astype(jnp.bfloat16)
    new_state = keep[:, None, None] * state + jnp.einsum(
        "hse,hsd->hed", value, scaled_key, preferred_element_type=jnp.float32
    )
    new_normal = keep[:, None] * normal + jnp.sum(scaled_key.astype(jnp.float32), axis=1)
    return ((new_state, new_normal, new_level), result)


def depthwise(extended, kernel):
    taps = kernel.shape[0]
    length = extended.shape[0] - taps + 1
    total = extended[0:length] * kernel[0]
    for index in range(1, taps):
        total = total + extended[index : index + length] * kernel[index]
    return total


def merge_states(first, second):
    first_state, first_normal, first_level, first_total = first
    second_state, second_normal, second_level, second_total = second
    shifted = first_level + second_total
    level = jnp.maximum(shifted, second_level)
    older = jnp.exp(shifted - level)
    newer = jnp.exp(second_level - level)
    state = older[:, None, None] * first_state + newer[:, None, None] * second_state
    normal = older[:, None] * first_normal + newer[:, None] * second_normal
    return (state, normal, level, first_total + second_total)


def on_device(
    tokens,
    conv_value_weight,
    conv_gate_weight,
    conv_kernel,
    conv_norm_gain,
    query_weight,
    key_weight,
    value_weight,
    input_gate_weight,
    forget_gate_weight,
    input_offset,
    forget_offset,
    memory_norm_gain,
    conv_out_weight,
    memory_out_weight,
):
    length = tokens.shape[0]
    heads_here = input_gate_weight.shape[1]
    whole = gather_directly(tokens, "tp", 1)
    gathered = sent_together(
        (conv_value_weight, conv_gate_weight, query_weight, key_weight, value_weight), SP, 0, 1
    )
    folded = tuple(
        (jnp.dot(whole, weight, preferred_element_type=jnp.float32) for weight in gathered)
    )
    conv_value, conv_gate, query_flat, key_flat, value_flat = folded
    gate_pre = jnp.dot(whole, input_gate_weight, preferred_element_type=jnp.float32)
    forget_pre = jnp.dot(whole, forget_gate_weight, preferred_element_type=jnp.float32)
    glu = (conv_value * jax.nn.sigmoid(conv_gate)).astype(jnp.bfloat16)
    taps = conv_kernel.shape[0]
    head_dim = query_flat.shape[1] // heads_here

    def to_heads(flat):
        return flat.astype(jnp.bfloat16).reshape(length, heads_here, head_dim).transpose(1, 0, 2)

    query = to_heads(query_flat)
    key = to_heads(key_flat)
    value = to_heads(value_flat)
    gate_in = (gate_pre + input_offset).T
    forget_log = jax.nn.log_sigmoid(forget_pre + forget_offset).T
    within = jnp.cumsum(forget_log, axis=1)
    total = within[:, -1]
    end_log = total[:, None] - within + gate_in
    local_level = jnp.max(end_log, axis=1)
    fresh = jnp.exp(end_log - local_level[:, None])
    scaled_key = (fresh[:, :, None] * key).astype(jnp.bfloat16)
    local_state = jnp.einsum("hse,hsd->hed", value, scaled_key, preferred_element_type=jnp.float32)
    local_normal = jnp.sum(scaled_key.astype(jnp.float32), axis=1)
    blank_state = (
        jnp.zeros_like(local_state),
        jnp.zeros_like(local_normal),
        jnp.full_like(local_level, LOWEST_LEVEL),
        jnp.zeros_like(total),
    )
    prior = shifted_2(glu[length - (taps - 1) :], SP, 1)
    incoming = entering(
        (local_state, local_normal, local_level, total), SP, merge_states, blank_state
    )
    extended = jnp.concatenate([prior, glu], axis=0).astype(jnp.float32)
    conv = depthwise(extended, conv_kernel.astype(jnp.float32))
    blocks = length // BLOCK

    def split(array):
        return jnp.moveaxis(array.reshape((heads_here, blocks, BLOCK) + array.shape[2:]), 1, 0)

    _, hidden = lax.scan(
        block_step,
        tuple(incoming[:3]),
        (split(query), split(key), split(value), split(gate_in), split(forget_log)),
    )
    hidden = jnp.moveaxis(hidden, 0, 1).reshape(heads_here, length, head_dim)
    hidden_squares = jnp.sum(hidden * hidden, axis=(0, 2))
    channel_sum, channel_squares, memory_squares = (
        of_everyone(jnp.sum(conv, axis=1), "tp"),
        of_everyone(jnp.sum(conv * conv, axis=1), "tp"),
        of_everyone(hidden_squares, "tp"),
    )
    channels = conv.shape[1] * lax.axis_size("tp")
    mean = (channel_sum / channels)[:, None]
    variance = (channel_squares / channels)[:, None] - mean * mean
    conv_branch = jax.nn.silu((conv - mean) * lax.rsqrt(variance + EPS) * conv_norm_gain).astype(
        jnp.bfloat16
    )
    entries = heads_here * head_dim * lax.axis_size("tp")
    memory_scale = lax.rsqrt(memory_squares / entries + EPS)
    hidden = hidden * memory_scale[None, :, None]
    hidden = hidden * memory_norm_gain.reshape(heads_here, 1, head_dim)
    memory_branch = (
        hidden.transpose(1, 0, 2).reshape(length, heads_here * head_dim).astype(jnp.bfloat16)
    )
    conv_columns, memory_columns = turned_gather((conv_out_weight, memory_out_weight), SP, (1, 1))
    contract = (((0,), (1,)), ((), ()))
    summed = sum_at_owner(
        (
            lax.dot_general(conv_columns, conv_branch, contract, preferred_element_type=jnp.float32)
            + lax.dot_general(
                memory_columns, memory_branch, contract, preferred_element_type=jnp.float32
            )
        ).astype(jnp.bfloat16),
        "tp",
        0,
    )
    return summed.T.astype(jnp.bfloat16)


def solution(mesh):
    split = Mesh(mesh.devices.reshape(16, 4, 2, mesh.shape["tp"]), ("sp_0", "sp_1", "sp_2", "tp"))
    in_specs = (
        P(SP, "tp"),
        P(SP, "tp"),
        P(SP, "tp"),
        P(None, "tp"),
        P("tp"),
        P(SP, "tp"),
        P(SP, "tp"),
        P(SP, "tp"),
        P(None, "tp"),
        P(None, "tp"),
        P(SP, "tp"),
        P(SP, "tp"),
        P("tp"),
        P("tp", SP),
        P("tp", SP),
    )
    out_specs = P(SP, "tp")
    return jax.shard_map(
        on_device, mesh=split, in_specs=in_specs, out_specs=out_specs, check_vma=False
    )
```

profile of v0, /device:TPU:1, one launch (start us, length us, event | category | flops | bytes accessed | tf_op | source)
XLA Modules:
  0.0 445.2 jit_solution(18037875826479777491)
XLA Ops:
  12.7 5.0 %all-to-all-start = ((bf16[4,128,512]{1,2,0:T(8,128)(2,1)}), bf16[4,128,512]{1,2,0:T(8,128)(2,1)S(1)}, u32[]{:S(2)}, u32[]{:S(2)}) async-start(bf16[4,128,512]{1,2,0:T(8,128)(2,1)} %broadcast_in_dim.26), calls=%async_computation | async-start | bytes 1048576 | tf_op jit(solution)/shard_map/all_to_all | solution.py:21
  17.7 1.3 dynamic-slice
  19.6 5.0 %all-to-all-done = bf16[4,128,512]{1,2,0:T(8,128)(2,1)S(1)} async-done(((bf16[4,128,512]{1,2,0:T(8,128)(2,1)}), bf16[4,128,512]{1,2,0:T(8,128)(2,1)S(1)}, u32[]{:S(2)}, u32[]{:S(2)}) %all-to-all-start) | async-done | bytes 524320 | tf_op jit(solution)/shard_map/all_to_all | solution.py:21
  27.7 8.5 %all-reduce.2 = (bf16[4]{0:T(256)(128)(2,1)S(1)}, bf16[4]{0:T(256)(128)(2,1)S(1)}) all-reduce(bf16[4]{0:T(256)(128)(2,1)S(1)} %dynamic-update-slice.1, bf16[4]{0:T(256)(128)(2,1)S(1)} %dynamic-update-slice), channel_id=3, replica_groups=mesh['sp_0'=16,'sp_1'=4,'sp_2'=2,'tp'=4] {'sp_2'}, use_global_device_ids=true, to_apply=%add.1 | all-reduce | flops 8 | bytes 32
  36.3 5.6 %all-gather.4 = bf16[4,1,2]{2,1,0:T(2,128)(2,1)S(1)} all-gather(bf16[1,1,2]{2,1,0:T(2,128)(2,1)S(1)} %get-tuple-element.249), channel_id=1, replica_groups=mesh['sp_0'=16,'sp_1'=4,'sp_2'=2,'tp'=4] {'sp_1'}, dimensions={0}, use_global_device_ids=true | all-gather | bytes 20 | tf_op jit(solution)/shard_map/all_gather | solution.py:55
  41.9 7.2 %all-gather.6 = bf16[4,1,2]{2,1,0:T(2,128)(2,1)S(1)} all-gather(bf16[1,1,2]{2,1,0:T(2,128)(2,1)S(1)} %get-tuple-element.250), channel_id=1, replica_groups=mesh['sp_0'=16,'sp_1'=4,'sp_2'=2,'tp'=4] {'sp_1'}, dimensions={0}, use_global_device_ids=true | all-gather | bytes 20 | tf_op jit(solution)/shard_map/all_gather | solution.py:55
  49.1 26.7 %all-gather.7 = bf16[16,1,2]{2,1,0:T(2,128)(2,1)S(1)} all-gather(bf16[1,1,2]{2,1,0:T(2,128)(2,1)S(1)} %get-tuple-element.238), channel_id=1, replica_groups=mesh['sp_0'=16,'sp_1'=4,'sp_2'=2,'tp'=4] {'sp_0'}, dimensions={0}, use_global_device_ids=true | all-gather | bytes 68 | tf_op jit(solution)/shard_map/all_gather | solution.py:55
  75.8 20.2 %all-gather.5 = bf16[16,1,2]{2,1,0:T(2,128)(2,1)S(1)} all-gather(bf16[1,1,2]{2,1,0:T(2,128)(2,1)S(1)} %get-tuple-element.239), channel_id=1, replica_groups=mesh['sp_0'=16,'sp_1'=4,'sp_2'=2,'tp'=4] {'sp_0'}, dimensions={0}, use_global_device_ids=true | all-gather | bytes 68 | tf_op jit(solution)/shard_map/all_gather | solution.py:55
  96.3 67.5 %all-gather.16.cloned.1.call-done = bf16[2048,2048]{1,0:T(8,128)(2,1)} async-done(((bf16[16,2048]{1,0:T(8,128)(2,1)}), bf16[2048,2048]{1,0:T(8,128)(2,1)}) %all-gather.16.cloned.1.call-update) | async-done | bytes 8388624 | tf_op jit(solution)/shard_map/all_gather | solution.py:34
  163.8 2.3 fusion.40
  166.4 2.4 fusion.37
  169.0 2.2 all-gather.2
  172.2 24.1 %all-gather.18.cloned.1.call-done = bf16[4,2,256,256]{3,2,1,0:T(8,128)(2,1)} async-done(((bf16[1,2,256,256]{3,2,1,0:T(8,128)(2,1)}), bf16[4,2,256,256]{3,2,1,0:T(8,128)(2,1)}) %all-gather.18.cloned.1.call-update) | async-done | bytes 1048592 | tf_op jit(solution)/shard_map/all_gather | solution.py:55
  196.3 2.2 fusion.66
  199.8 4.2 all-gather.8
  204.1 6.5 %all_gather.72 = bf16[4,2,256]{2,1,0:T(2,128)(2,1)S(1)} all-gather(bf16[1,2,256]{2,1,0:T(2,128)(2,1)S(1)} %fusion.217), channel_id=1, replica_groups=mesh['sp_0'=16,'sp_1'=4,'sp_2'=2,'tp'=4] {'sp_1'}, dimensions={0}, use_global_device_ids=true | all-gather | bytes 5120 | tf_op jit(solution)/shard_map/all_gather | solution.py:55
  210.5 1.6 fusion.55
  212.1 1.6 fusion.51
  213.7 4.5 %collective-permute-start = (bf16[30,256]{1,0:T(8,128)(2,1)S(1)}, bf16[30,256]{1,0:T(8,128)(2,1)S(1)}, u32[]{:S(2)}, u32[]{:S(2)}) collective-permute-start(bf16[30,256]{1,0:T(8,128)(2,1)S(1)} %slice.672), channel_id=1, source_target_pairs={{0,4},{4,8},{8,12},{12,16},{16,20},{20,24},{24,28},{28,32},{32,36}... | collective-permute-start | bytes 46088 | tf_op jit(solution)/shard_map/ppermute | solution.py:40
  218.2 2.4 fusion.43
  221.9 4.0 all-to-all-start.2
  225.9 25.9 %all_gather.73 = bf16[16,2,256]{2,1,0:T(2,128)(2,1)S(1)} all-gather(bf16[1,2,256]{2,1,0:T(2,128)(2,1)S(1)} %fusion.182), channel_id=1, replica_groups=mesh['sp_0'=16,'sp_1'=4,'sp_2'=2,'tp'=4] {'sp_0'}, dimensions={0}, use_global_device_ids=true | all-gather | bytes 17408 | tf_op jit(solution)/shard_map/all_gather | solution.py:55
  252.3 4.6 %all-to-all-start.1 = ((f32[4,1,128]{2,1,0:T(1,128)}), f32[4,1,128]{2,1,0:T(1,128)S(1)}, u32[]{:S(2)}, u32[]{:S(2)}) async-start(f32[4,1,128]{2,1,0:T(1,128)} %broadcast_in_dim.27), calls=%async_computation.1 | async-start | bytes 4096 | tf_op jit(solution)/shard_map/all_to_all | solution.py:21
  257.3 3.9 all-to-all-done.1
  261.2 9.4 %all-gather.20.cloned.1.call-done = bf16[16,2,256,256]{3,2,1,0:T(8,128)(2,1)} async-done(((bf16[1,2,256,256]{3,2,1,0:T(8,128)(2,1)}), bf16[16,2,256,256]{3,2,1,0:T(8,128)(2,1)}) %all-gather.20.cloned.1.call-update) | async-done | bytes 4194320 | tf_op jit(solution)/shard_map/all_gather | solution.py:55
  270.6 4.5 %fusion.78 = f32[2,256,256]{2,1,0:T(8,128)S(1)} fusion(bf16[16,2,256,256]{3,2,1,0:T(8,128)(2,1)} %all-gather.20.cloned.1.call-done, f32[2]{0:T(128)S(1)} %get-tuple-element.247, f32[2]{0:T(128)S(1)} %get-tuple-element.241, f32[2]{0:T(128)S(1)} %get-tuple-element.246, f32[2]{0:T(128)S(1)} %get-tuple-element.245, f32[2]{0:T(128)S(1)} %get-tuple-element.240, ...), kind=kLoop, calls=%fused_computation.107 | loop fusion | flops 15073280 | bytes 6291878 | tf_op jit(solution)/shard_map/add | solution.py:151
  275.1 4.7 %while.16 = (s32[]{:T(128)}, f32[2,256,256]{2,1,0:T(8,128)S(1)}, f32[2,256]{1,0:T(2,128)S(1)}, f32[2]{0:T(128)S(1)}, f32[2,2,64,256]{3,2,0,1:T(8,128)S(1)}, /*in...) while((s32[]{:T(128)}, f32[2,256,256]{2,1,0:T(8,128)S(1)}, ...), condition=%wide.region_13.14_spmd, body=%wide.region_7.13_spmd.sunk | while | flops 42875268 | bytes 2589965 | solution.py:222
  280.6 4.0 all-to-all-start.3
  284.6 136.1 %all-gather.14.cloned.1.call-done = bf16[2048,768]{1,0:T(8,128)(2,1)} async-done(((bf16[16,768]{1,0:T(8,128)(2,1)}), bf16[2048,768]{1,0:T(8,128)(2,1)}) %all-gather.14.cloned.1.call-update) | async-done | bytes 3145744 | tf_op jit(solution)/shard_map/all_gather | solution.py:77
  420.7 1.7 fusion.57
  422.7 2.3 fusion.29
  425.0 12.8 %all_to_all.28 = bf16[4,512,128]{2,1,0:T(8,128)(2,1)S(1)} all-to-all(bf16[4,512,128]{2,1,0:T(8,128)(2,1)S(1)} %bitcast.981), channel_id=1, replica_groups=mesh['sp_0'=16,'sp_1'=4,'sp_2'=2,'tp'=4] {'tp'}, dimensions={0} | all-to-all | bytes 1048576 | tf_op jit(solution)/shard_map/all_to_all | solution.py:92
  (127 shorter events, 21.0 us)
Async XLA Ops:
  6.5 19.5 %copy-start = (bf16[2048,2]{0,1:T(2,128)(2,1)S(1)}, bf16[2048,2]{0,1:T(2,128)(2,1)}, u32[]{:S(2)}) copy-start(bf16[2048,2]{0,1:T(2,128)(2,1)} %param.25) | copy-start | bytes 24580
  6.5 157.3 %all-gather.16.cloned.1.call-start = ((), (), s32[]{:S(2)}) async-start(), calls=%async_computation.6 | async-start | bytes 8454144 | tf_op jit(solution)/shard_map/all_gather | solution.py:34
  10.1 0.6 copy-start.2
  12.7 11.9 %all-to-all-start = ((bf16[4,128,512]{1,2,0:T(8,128)(2,1)}), bf16[4,128,512]{1,2,0:T(8,128)(2,1)S(1)}, u32[]{:S(2)}, u32[]{:S(2)}) async-start(bf16[4,128,512]{1,2,0:T(8,128)(2,1)} %broadcast_in_dim.26), calls=%async_computation | async-start | bytes 1048576 | tf_op jit(solution)/shard_map/all_to_all | solution.py:21
  17.7 178.6 %all-gather.18.cloned.1.call-start = ((), (), s32[]{:S(2)}) async-start(), calls=%async_computation.7 | async-start | bytes 1310720 | tf_op jit(solution)/shard_map/all_gather | solution.py:55
  166.3 32.3 %copy-start.4 = (bf16[512,16]{0,1:T(8,128)(2,1)S(1)}, bf16[512,16]{0,1:T(8,128)(2,1)}, u32[]{:S(2)}) copy-start(bf16[512,16]{0,1:T(8,128)(2,1)} %param.31) | copy-start | bytes 49156
  166.3 32.3 %copy-start.5 = (bf16[256,16]{0,1:T(8,128)(2,1)S(1)}, bf16[256,16]{0,1:T(8,128)(2,1)}, u32[]{:S(2)}) copy-start(bf16[256,16]{0,1:T(8,128)(2,1)} %param.30) | copy-start | bytes 24580
  166.3 32.9 %copy-start.3 = (bf16[31,256]{1,0:T(8,128)(2,1)S(1)}, bf16[31,256]{1,0:T(8,128)(2,1)}, u32[]{:S(2)}) copy-start(bf16[31,256]{1,0:T(8,128)(2,1)} %param.20) | copy-start | bytes 47620
  166.3 33.0 %copy-start.6 = (f32[512]{0:T(512)S(1)}, f32[512]{0:T(512)}, u32[]{:S(2)}) copy-start(f32[512]{0:T(512)} %param.29) | copy-start | bytes 6148
  172.1 98.4 %all-gather.20.cloned.1.call-start = ((), (), s32[]{:S(2)}) async-start(), calls=%async_computation.8 | async-start | bytes 4456448 | tf_op jit(solution)/shard_map/all_gather | solution.py:55
  198.6 222.1 %all-gather.14.cloned.1.call-start = ((), (), s32[]{:S(2)}) async-start(), calls=%async_computation.5 | async-start | bytes 3170304 | tf_op jit(solution)/shard_map/all_gather | solution.py:77
  213.7 56.9 %copy-start.1 = (bf16[4,2,256,256]{3,2,1,0:T(8,128)(2,1)S(1)}, bf16[4,2,256,256]{3,2,1,0:T(8,128)(2,1)}, u32[]{:S(2)}) copy-start(bf16[4,2,256,256]{3,2,1,0:T(8,128)(2,1)} %all-gather.18.cloned.1.call-done) | copy-start | bytes 3145732
  213.7 7.0 %collective-permute-start = (bf16[30,256]{1,0:T(8,128)(2,1)S(1)}, bf16[30,256]{1,0:T(8,128)(2,1)S(1)}, u32[]{:S(2)}, u32[]{:S(2)}) collective-permute-start(bf16[30,256]{1,0:T(8,128)(2,1)S(1)} %slice.672), channel_id=1, source_target_pairs={{0,4},{4,8},{8,12},{12,16},{16,20},{20,24},{24,28},{28,32},{32,36}... | collective-permute-start | bytes 46088 | tf_op jit(solution)/shard_map/ppermute | solution.py:40
  221.9 29.9 %all-to-all-start.2 = ((f32[4,1,128]{2,1,0:T(1,128)}), f32[4,1,128]{2,1,0:T(1,128)S(1)}, u32[]{:S(2)}, u32[]{:S(2)}) async-start(f32[4,1,128]{2,1,0:T(1,128)} %broadcast_in_dim.28), calls=%async_computation.2 | async-start | bytes 4096 | tf_op jit(solution)/shard_map/all_to_all | solution.py:21
  252.3 8.9 %all-to-all-start.1 = ((f32[4,1,128]{2,1,0:T(1,128)}), f32[4,1,128]{2,1,0:T(1,128)S(1)}, u32[]{:S(2)}, u32[]{:S(2)}) async-start(f32[4,1,128]{2,1,0:T(1,128)} %broadcast_in_dim.27), calls=%async_computation.1 | async-start | bytes 4096 | tf_op jit(solution)/shard_map/all_to_all | solution.py:21
  275.1 145.6 %copy-start.7 = (f32[256]{0:T(256)S(1)}, f32[256]{0:T(256)}, u32[]{:S(2)}) copy-start(f32[256]{0:T(256)} %param.21) | copy-start | bytes 3076
  280.6 141.8 %all-to-all-start.3 = ((f32[4,1,128]{2,1,0:T(1,128)}), f32[4,1,128]{2,1,0:T(1,128)S(1)}, u32[]{:S(2)}, u32[]{:S(2)}) async-start(f32[4,1,128]{2,1,0:T(1,128)} %broadcast_in_dim.33), calls=%async_computation.3 | async-start | bytes 4096 | tf_op jit(solution)/shard_map/all_to_all | solution.py:21
Sparse Core Ops, SparseCore 0:
  10.9 152.9 all-gather.15
  172.3 24.0 all-gather.17
  198.7 71.8 all-gather.19
  273.6 147.0 all-gather.13
where the time goes:
time: 446 us; the launch traced here: 445 us
  waiting for transfers between devices  246 us (55%)
  blocking collectives  120 us (27%)
  starting transfers between devices  22.2 us (5%)
  matrix products  18.6 us (4%)
  between operations  14.1 us (3%)
  other arithmetic  12.5 us (3%)
  local copies, waits for them, and re-layouts  12 us (3%)
    all_gather x1, waiting for transfers between devices, turned_gather(): out, at, finished = (lax.all_gather(both, axis, axis=0, tiled=True), 0, [])  136 us
    all_gather x8, blocking collectives, entering(): lax.all_gather(part.astype(kind), axis)  98.4 us
    all_gather x1, waiting for transfers between devices, sent_together(): lax.all_gather(both, axis, axis=dim, tiled=True)  67.5 us
    all_gather x2, waiting for transfers between devices, entering(): lax.all_gather(part.astype(kind), axis)  33.5 us
    all_to_all x4, starting transfers between devices, copy_for_each(): return lax.all_to_all(copies, axis, split_axis=0, concat_axis=0, tiled=True)  17.6 us
    all_to_all x1, blocking collectives, sum_at_owner(): lax.all_to_all(blocks, axis, split_axis=0, concat_axis=0, tiled=True)  12.8 us
    dot_general x5, matrix products, on_device(): jnp.dot(whole, weight, preferred_element_type=jnp.float32)  10.2 us
  transfers between devices with their start and end apart: 9, of which 6 were waited for; matrix products, arithmetic and copies ran while one was open for 6% of the time, Pallas kernels for 0%

commit v1 on v0

--- a/solution.py
+++ b/solution.py
@@ -8,6 +8,11 @@
 SP = ("sp_0", "sp_1", "sp_2")
 EPS = 1e-06
 LOWEST_LEVEL = -1e30
+
+
+def exchange_gather(x, axis, dim):
+    sent = jnp.stack([x] * lax.axis_size(axis))
+    return jnp.concatenate(lax.all_to_all(sent, axis, 0, 0), axis=dim)
 
 
 def in_order(blocks, dim):
@@ -74,7 +79,7 @@
 def turned_gather(arrays, axis, dims):
     turned = [jnp.moveaxis(a, dim, 0) for a, dim in zip(arrays, dims)]
     both = jnp.concatenate([t.reshape(len(t), -1) for t in turned], axis=1)
-    out, at, finished = (lax.all_gather(both, axis, axis=0, tiled=True), 0, [])
+    out, at, finished = (exchange_gather(both, axis, 0), 0, [])
     for t, dim in zip(turned, dims):
         share = out[:, at : at + t[0].size].reshape(-1, *t.shape[1:])
         finished.append(jnp.moveaxis(share, 0, dim))

time: 446 us -> 467 us (1.047); the launches traced: 445 us -> 458 us
  waiting for transfers between devices: 246 us -> 104 us
  blocking collectives: 120 us -> 256 us
  starting transfers between devices: 22.2 us -> 39.4 us
    all_gather x1 -> x0, waiting for transfers between devices: 136 us -> none  [turned_gather(): out, at, finished = (lax.all_gather(both, axis, axis=0, tiled=True), 0, [])]
    all_gather x8, blocking collectives: 98.4 us -> 231 us  [entering(): lax.all_gather(part.astype(kind), axis)]
    all_to_all x0 -> x1, starting transfers between devices: none -> 22.2 us  [exchange_gather(): return jnp.concatenate(lax.all_to_all(sent, axis, 0, 0), axis=dim)]
    all_gather x2, waiting for transfers between devices: 33.5 us -> 24.1 us  [entering(): lax.all_gather(part.astype(kind), axis)]
    all_to_all x0 -> x1, blocking collectives: none -> 7.94 us  [copy_for_each(): return lax.all_to_all(copies, axis, split_axis=0, concat_axis=0, tiled=True)]
    all_to_all x4 -> x3, starting transfers between devices: 17.6 us -> 12.5 us  [copy_for_each(): return lax.all_to_all(copies, axis, split_axis=0, concat_axis=0, tiled=True)]
    all_to_all x4 -> x3, waiting for transfers between devices: 8.85 us -> 11.4 us  [copy_for_each(): return lax.all_to_all(copies, axis, split_axis=0, concat_axis=0, tiled=True)]
  transfers between devices with their start and end apart: 9 -> 8, of which waited for: 6 -> 6; matrix products, arithmetic and copies ran while one was open for 6% -> 6% of each run, Pallas kernels for 0% -> 0%
where the time goes in v1:
time: 467 us; the launch traced here: 458 us
  blocking collectives  256 us (55%)
  waiting for transfers between devices  104 us (22%)
  starting transfers between devices  39.4 us (8%)
  matrix products  18.8 us (4%)
  between operations  14.1 us (3%)
  local copies, waits for them, and re-layouts  13.3 us (3%)
  other arithmetic  12 us (3%)
    all_gather x8, blocking collectives, entering(): lax.all_gather(part.astype(kind), axis)  231 us
    all_gather x1, waiting for transfers between devices, sent_together(): lax.all_gather(both, axis, axis=dim, tiled=True)  67.5 us
    all_gather x2, waiting for transfers between devices, entering(): lax.all_gather(part.astype(kind), axis)  24.1 us
    all_to_all x1, starting transfers between devices, exchange_gather(): return jnp.concatenate(lax.all_to_all(sent, axis, 0, 0), axis=dim)  22.2 us
    all_to_all x3, starting transfers between devices, copy_for_each(): return lax.all_to_all(copies, axis, split_axis=0, concat_axis=0, tiled=True)  12.5 us
    all_to_all x3, waiting for transfers between devices, copy_for_each(): return lax.all_to_all(copies, axis, split_axis=0, concat_axis=0, tiled=True)  11.4 us
    dot_general x5, matrix products, on_device(): jnp.dot(whole, weight, preferred_element_type=jnp.float32)  10.4 us
  transfers between devices with their start and end apart: 8, of which 6 were waited for; matrix products, arithmetic and copies ran while one was open for 6% of the time, Pallas kernels for 0%

profile of v1, /device:TPU:1, one launch (start us, length us, event | category | flops | bytes accessed | tf_op | source)
XLA Modules:
  0.0 458.0 jit_solution(9289053608185997120)
XLA Ops:
  12.7 5.0 %all-to-all-start.1 = ((bf16[4,128,512]{1,2,0:T(8,128)(2,1)}), bf16[4,128,512]{1,2,0:T(8,128)(2,1)S(1)}, u32[]{:S(2)}, u32[]{:S(2)}) async-start(bf16[4,128,512]{1,2,0:T(8,128)(2,1)} %broadcast_in_dim.26), calls=%async_computation.1 | async-start | bytes 1048576 | tf_op jit(solution)/shard_map/all_to_all | solution.py:26
  19.6 5.0 %all-to-all-done.1 = bf16[4,128,512]{1,2,0:T(8,128)(2,1)S(1)} async-done(((bf16[4,128,512]{1,2,0:T(8,128)(2,1)}), bf16[4,128,512]{1,2,0:T(8,128)(2,1)S(1)}, u32[]{:S(2)}, u32[]{:S(2)}) %all-to-all-start.1) | async-done | bytes 524320 | tf_op jit(solution)/shard_map/all_to_all | solution.py:26
  27.7 8.5 %all-reduce.2 = (bf16[4]{0:T(256)(128)(2,1)S(1)}, bf16[4]{0:T(256)(128)(2,1)S(1)}) all-reduce(bf16[4]{0:T(256)(128)(2,1)S(1)} %dynamic-update-slice.1, bf16[4]{0:T(256)(128)(2,1)S(1)} %dynamic-update-slice), channel_id=3, replica_groups=mesh['sp_0'=16,'sp_1'=4,'sp_2'=2,'tp'=4] {'sp_2'}, use_global_device_ids=true, to_apply=%add.1 | all-reduce | flops 8 | bytes 32
  36.3 5.6 %all-gather.4 = bf16[4,1,2]{2,1,0:T(2,128)(2,1)S(1)} all-gather(bf16[1,1,2]{2,1,0:T(2,128)(2,1)S(1)} %get-tuple-element.249), channel_id=1, replica_groups=mesh['sp_0'=16,'sp_1'=4,'sp_2'=2,'tp'=4] {'sp_1'}, dimensions={0}, use_global_device_ids=true | all-gather | bytes 20 | tf_op jit(solution)/shard_map/all_gather | solution.py:60
  41.9 7.2 %all-gather.6 = bf16[4,1,2]{2,1,0:T(2,128)(2,1)S(1)} all-gather(bf16[1,1,2]{2,1,0:T(2,128)(2,1)S(1)} %get-tuple-element.250), channel_id=1, replica_groups=mesh['sp_0'=16,'sp_1'=4,'sp_2'=2,'tp'=4] {'sp_1'}, dimensions={0}, use_global_device_ids=true | all-gather | bytes 20 | tf_op jit(solution)/shard_map/all_gather | solution.py:60
  49.1 26.7 %all-gather.7 = bf16[16,1,2]{2,1,0:T(2,128)(2,1)S(1)} all-gather(bf16[1,1,2]{2,1,0:T(2,128)(2,1)S(1)} %get-tuple-element.238), channel_id=1, replica_groups=mesh['sp_0'=16,'sp_1'=4,'sp_2'=2,'tp'=4] {'sp_0'}, dimensions={0}, use_global_device_ids=true | all-gather | bytes 68 | tf_op jit(solution)/shard_map/all_gather | solution.py:60
  75.8 20.2 %all-gather.5 = bf16[16,1,2]{2,1,0:T(2,128)(2,1)S(1)} all-gather(bf16[1,1,2]{2,1,0:T(2,128)(2,1)S(1)} %get-tuple-element.239), channel_id=1, replica_groups=mesh['sp_0'=16,'sp_1'=4,'sp_2'=2,'tp'=4] {'sp_0'}, dimensions={0}, use_global_device_ids=true | all-gather | bytes 68 | tf_op jit(solution)/shard_map/all_gather | solution.py:60
  96.3 67.5 %all-gather.13.cloned.1.call-done = bf16[2048,2048]{1,0:T(8,128)(2,1)} async-done(((bf16[16,2048]{1,0:T(8,128)(2,1)}), bf16[2048,2048]{1,0:T(8,128)(2,1)}) %all-gather.13.cloned.1.call-update) | async-done | bytes 8388624 | tf_op jit(solution)/shard_map/all_gather | solution.py:39
  163.8 2.3 fusion.40
  166.3 2.4 fusion.37
  169.0 2.2 all-gather.2
  172.2 24.1 %all-gather.15.cloned.1.call-done = bf16[4,2,256,256]{3,2,1,0:T(8,128)(2,1)} async-done(((bf16[1,2,256,256]{3,2,1,0:T(8,128)(2,1)}), bf16[4,2,256,256]{3,2,1,0:T(8,128)(2,1)}) %all-gather.15.cloned.1.call-update) | async-done | bytes 1048592 | tf_op jit(solution)/shard_map/all_gather | solution.py:60
  196.3 2.2 fusion.66
  198.6 1.6 fusion.55
  200.2 1.6 fusion.51
  201.8 4.6 %collective-permute-start = (bf16[30,256]{1,0:T(8,128)(2,1)S(1)}, bf16[30,256]{1,0:T(8,128)(2,1)S(1)}, u32[]{:S(2)}, u32[]{:S(2)}) collective-permute-start(bf16[30,256]{1,0:T(8,128)(2,1)S(1)} %slice.672), channel_id=1, source_target_pairs={{0,4},{4,8},{8,12},{12,16},{16,20},{20,24},{24,28},{28,32},{32,36}... | collective-permute-start | bytes 46088 | tf_op jit(solution)/shard_map/ppermute | solution.py:45
  207.9 7.9 %all_to_all.33 = f32[4,1,128]{2,1,0:T(1,128)S(1)} all-to-all(f32[4,1,128]{2,1,0:T(1,128)S(1)} %broadcast_in_dim.28), channel_id=1, replica_groups=mesh['sp_0'=16,'sp_1'=4,'sp_2'=2,'tp'=4] {'tp'}, dimensions={0} | all-to-all | bytes 4096 | tf_op jit(solution)/shard_map/all_to_all | solution.py:26
  216.4 3.2 all-to-all-start.2
  219.7 4.1 all-to-all-done.2
  223.8 1.9 stack.2
  225.6 22.2 %all-to-all-start = ((bf16[128,16,768]{2,1,0:T(8,128)(2,1)}), bf16[128,16,768]{2,1,0:T(8,128)(2,1)}, u32[]{:S(2)}, u32[]{:S(2)}) async-start(bf16[128,16,768]{2,1,0:T(8,128)(2,1)} %stack.2), calls=%async_computation | async-start | bytes 6291456 | tf_op jit(solution)/shard_map/all_to_all | solution.py:15
  248.3 2.5 fusion.43
  251.0 2.4 all-gather.8
  253.5 8.0 %all_gather.68 = bf16[4,2,256]{2,1,0:T(2,128)(2,1)S(1)} all-gather(bf16[1,2,256]{2,1,0:T(2,128)(2,1)S(1)} %fusion.217), channel_id=1, replica_groups=mesh['sp_0'=16,'sp_1'=4,'sp_2'=2,'tp'=4] {'sp_1'}, dimensions={0}, use_global_device_ids=true | all-gather | bytes 5120 | tf_op jit(solution)/shard_map/all_gather | solution.py:60
  261.6 158.3 %all_gather.69 = bf16[16,2,256]{2,1,0:T(2,128)(2,1)S(1)} all-gather(bf16[1,2,256]{2,1,0:T(2,128)(2,1)S(1)} %fusion.182), channel_id=1, replica_groups=mesh['sp_0'=16,'sp_1'=4,'sp_2'=2,'tp'=4] {'sp_0'}, dimensions={0}, use_global_device_ids=true | all-gather | bytes 17408 | tf_op jit(solution)/shard_map/all_gather | solution.py:60
  420.2 4.7 %fusion.78 = f32[2,256,256]{2,1,0:T(8,128)S(1)} fusion(bf16[16,2,256,256]{3,2,1,0:T(8,128)(2,1)} %all-gather.17.cloned.1.call-done, f32[2]{0:T(128)S(1)} %get-tuple-element.247, f32[2]{0:T(128)S(1)} %get-tuple-element.241, f32[2]{0:T(128)S(1)} %get-tuple-element.246, f32[2]{0:T(128)S(1)} %get-tuple-element.245, f32[2]{0:T(128)S(1)} %get-tuple-element.240, ...), kind=kLoop, calls=%fused_computation.107 | loop fusion | flops 15073280 | bytes 6291878 | tf_op jit(solution)/shard_map/add | solution.py:156
  424.9 4.7 %while.16 = (s32[]{:T(128)}, f32[2,256,256]{2,1,0:T(8,128)S(1)}, f32[2,256]{1,0:T(2,128)S(1)}, f32[2]{0:T(128)S(1)}, f32[2,2,64,256]{3,2,0,1:T(8,128)S(1)}, /*in...) while((s32[]{:T(128)}, f32[2,256,256]{2,1,0:T(8,128)S(1)}, ...), condition=%wide.region_13.14_spmd, body=%wide.region_7.13_spmd.sunk | while | flops 42875268 | bytes 2589965 | solution.py:227
  430.4 4.3 all-to-all-start.4
  434.7 1.7 fusion.57
  436.4 2.3 all-to-all-done.4
  439.0 2.3 fusion.29
  441.3 9.3 %all_to_all.34 = bf16[4,512,128]{2,1,0:T(8,128)(2,1)S(1)} all-to-all(bf16[4,512,128]{2,1,0:T(8,128)(2,1)S(1)} %bitcast.982), channel_id=1, replica_groups=mesh['sp_0'=16,'sp_1'=4,'sp_2'=2,'tp'=4] {'tp'}, dimensions={0} | all-to-all | bytes 1048576 | tf_op jit(solution)/shard_map/all_to_all | solution.py:97
  (126 shorter events, 21.8 us)
Async XLA Ops:
  6.5 19.5 %copy-start = (bf16[2048,2]{0,1:T(2,128)(2,1)S(1)}, bf16[2048,2]{0,1:T(2,128)(2,1)}, u32[]{:S(2)}) copy-start(bf16[2048,2]{0,1:T(2,128)(2,1)} %param.25) | copy-start | bytes 24580
  6.5 157.3 %all-gather.13.cloned.1.call-start = ((), (), s32[]{:S(2)}) async-start(), calls=%async_computation.6 | async-start | bytes 8454144 | tf_op jit(solution)/shard_map/all_gather | solution.py:39
  10.1 0.6 copy-start.2
  12.7 11.9 %all-to-all-start.1 = ((bf16[4,128,512]{1,2,0:T(8,128)(2,1)}), bf16[4,128,512]{1,2,0:T(8,128)(2,1)S(1)}, u32[]{:S(2)}, u32[]{:S(2)}) async-start(bf16[4,128,512]{1,2,0:T(8,128)(2,1)} %broadcast_in_dim.26), calls=%async_computation.1 | async-start | bytes 1048576 | tf_op jit(solution)/shard_map/all_to_all | solution.py:26
  17.7 178.6 %all-gather.15.cloned.1.call-start = ((), (), s32[]{:S(2)}) async-start(), calls=%async_computation.7 | async-start | bytes 1310720 | tf_op jit(solution)/shard_map/all_gather | solution.py:60
  168.7 29.9 %copy-start.3 = (bf16[31,256]{1,0:T(8,128)(2,1)S(1)}, bf16[31,256]{1,0:T(8,128)(2,1)}, u32[]{:S(2)}) copy-start(bf16[31,256]{1,0:T(8,128)(2,1)} %param.20) | copy-start | bytes 47620
  172.1 248.1 %all-gather.17.cloned.1.call-start = ((), (), s32[]{:S(2)}) async-start(), calls=%async_computation.8 | async-start | bytes 4456448 | tf_op jit(solution)/shard_map/all_gather | solution.py:60
  200.2 19.5 %copy-start.4 = (bf16[512,16]{0,1:T(8,128)(2,1)S(1)}, bf16[512,16]{0,1:T(8,128)(2,1)}, u32[]{:S(2)}) copy-start(bf16[512,16]{0,1:T(8,128)(2,1)} %param.31) | copy-start | bytes 49156
  200.2 19.5 %copy-start.5 = (bf16[256,16]{0,1:T(8,128)(2,1)S(1)}, bf16[256,16]{0,1:T(8,128)(2,1)}, u32[]{:S(2)}) copy-start(bf16[256,16]{0,1:T(8,128)(2,1)} %param.30) | copy-start | bytes 24580
  201.8 5.4 %collective-permute-start = (bf16[30,256]{1,0:T(8,128)(2,1)S(1)}, bf16[30,256]{1,0:T(8,128)(2,1)S(1)}, u32[]{:S(2)}, u32[]{:S(2)}) collective-permute-start(bf16[30,256]{1,0:T(8,128)(2,1)S(1)} %slice.672), channel_id=1, source_target_pairs={{0,4},{4,8},{8,12},{12,16},{16,20},{20,24},{24,28},{28,32},{32,36}... | collective-permute-start | bytes 46088 | tf_op jit(solution)/shard_map/ppermute | solution.py:45
  216.4 7.4 %all-to-all-start.2 = ((f32[4,1,128]{2,1,0:T(1,128)}), f32[4,1,128]{2,1,0:T(1,128)S(1)}, u32[]{:S(2)}, u32[]{:S(2)}) async-start(f32[4,1,128]{2,1,0:T(1,128)} %broadcast_in_dim.27), calls=%async_computation.2 | async-start | bytes 4096 | tf_op jit(solution)/shard_map/all_to_all | solution.py:26
  225.6 22.2 %copy-start.6 = (f32[512]{0:T(512)S(1)}, f32[512]{0:T(512)}, u32[]{:S(2)}) copy-start(f32[512]{0:T(512)} %param.29) | copy-start | bytes 6148
  225.6 204.1 %all-to-all-start = ((bf16[128,16,768]{2,1,0:T(8,128)(2,1)}), bf16[128,16,768]{2,1,0:T(8,128)(2,1)}, u32[]{:S(2)}, u32[]{:S(2)}) async-start(bf16[128,16,768]{2,1,0:T(8,128)(2,1)} %stack.2), calls=%async_computation | async-start | bytes 6291456 | tf_op jit(solution)/shard_map/all_to_all | solution.py:15
  248.1 172.1 %copy-start.1 = (bf16[4,2,256,256]{3,2,1,0:T(8,128)(2,1)S(1)}, bf16[4,2,256,256]{3,2,1,0:T(8,128)(2,1)}, u32[]{:S(2)}) copy-start(bf16[4,2,256,256]{3,2,1,0:T(8,128)(2,1)} %all-gather.15.cloned.1.call-done) | copy-start | bytes 3145732
  424.9 9.8 %copy-start.7 = (f32[256]{0:T(256)S(1)}, f32[256]{0:T(256)}, u32[]{:S(2)}) copy-start(f32[256]{0:T(256)} %param.21) | copy-start | bytes 3076
  430.4 8.4 %all-to-all-start.4 = ((f32[4,1,128]{2,1,0:T(1,128)}), f32[4,1,128]{2,1,0:T(1,128)S(1)}, u32[]{:S(2)}, u32[]{:S(2)}) async-start(f32[4,1,128]{2,1,0:T(1,128)} %broadcast_in_dim.33), calls=%async_computation.4 | async-start | bytes 4096 | tf_op jit(solution)/shard_map/all_to_all | solution.py:26
Sparse Core Ops, SparseCore 0:
  10.9 152.9 all-gather.12
  172.2 24.0 all-gather.14
  198.7 142.0 all-gather.16
